TPU v7x, 512 devices: a whole 4x8x8 slice. The times are simulated.
512 devices in a mesh: sp: 64 (over z, y), tp: 4 (over x), dp: 2 (over core).
Axes of the slice: x: 4, y: 8, z: 8, core: 2. Of those that a mesh axis runs over, the one named last changes fastest.
Arguments:
- latent: bfloat16 [2, 16384, 2048], P('dp', ('sp', 'tp')), may hold values from -6 to 6
- condition: bfloat16 [2, 2048], P('dp', ('sp', 'tp')), may hold values from -6 to 6
- context: bfloat16 [2, 512, 2048], P('dp', 'sp'), may hold values from -6 to 6
- context_vector: bfloat16 [2048], P(('sp', 'tp')), may hold values from -6 to 6
- modulator: bfloat16 [2048, 6144], P(('sp', 'tp')), may hold values from -0.3125 to 0.3125
- norm_gain: float32 [2048], replicated, may hold values from 0.1 to 1.9
- query_weight: bfloat16 [2048, 512], P(None, 'tp'), may hold values from -4 to 4
- key_weight: bfloat16 [2048, 512], P(None, 'tp'), may hold values from -0.125 to 0.125
- value_weight: bfloat16 [2048, 512], P(None, 'tp'), may hold values from -0.125 to 0.125
- head_gain: float32 [128], replicated, may hold values from 0.1 to 1.9
- lambdas: float32 [4], P('tp'), may hold values from 0.3 to 0.8
- context_bias: float32 [4, 2], P('tp'), may hold values from 1.3 to 2.7
- out_weight: bfloat16 [512, 2048], P('tp'), may hold values from -0.25 to 0.25
Outputs:
- updated: bfloat16 [2, 16384, 2048], P('dp', ('sp', 'tp'))
All inputs are finite; a program needn't handle non-finite values.
Results may differ from a plain program's by a relative error of at most 0.024.
Values may be sent and summed in bfloat16 or wider, within the bound.
A program may use at most 64 MiB of HBM per device.

v0:
```python
import jax
import jax.numpy as jnp
from jax import lax
from jax.sharding import Mesh
from jax.sharding import PartitionSpec as P

SP_TP = ("sp_0", "sp_1", "tp")
SP = ("sp_0", "sp_1")


EPSILON = 1e-06
OUT_SCALE = 0.8
KEY_BLOCK = 2048
LOW_START = -1e30


def by_axis(shard, axes):
    for axis in axes:
        shard = lax.psum(shard, axis)
    return shard


def joined_along(blocks, dim):
    lengths = list(blocks.shape[1:])
    lengths[dim] *= blocks.shape[0]
    return jnp.moveaxis(blocks, 0, dim).reshape(lengths)


def sent_to_all(shard, axis):
    copies = jnp.broadcast_to(shard, (lax.axis_size(axis), *shard.shape))
    return lax.all_to_all(copies, axis, split_axis=0, concat_axis=0, tiled=True)


def gather_directly(shard, axis, dim):
    return joined_along(sent_to_all(shard, axis), dim)


def sent_together(arrays, axis, dim, along):
    ends, at = ([], 0)
    for a in arrays[:-1]:
        at += a.shape[along]
        ends.append(at)
    both = jnp.concatenate(arrays, axis=along)
    return tuple(jnp.split(lax.all_gather(both, axis, axis=dim, tiled=True), ends, axis=along))


def split_up(shard, dim, devices):
    lengths = shard.shape
    blocks = shard.reshape(*lengths[:dim], devices, lengths[dim] // devices, *lengths[dim + 1 :])
    return jnp.moveaxis(blocks, dim, 0)


def summed_on_arrival(shard, axis, dim):
    blocks = split_up(shard, dim, lax.axis_size(axis))
    arrived = lax.all_to_all(blocks, axis, split_axis=0, concat_axis=0, tiled=True)
    return arrived.astype(jnp.float32).sum(axis=0)


def modulate(inputs, gain_vector, shift_vector, scale_vector):
    as_float = inputs.astype(jnp.float32)
    normed = as_float * lax.rsqrt(jnp.mean(as_float * as_float, axis=-1, keepdims=True) + EPSILON)
    return (normed * gain_vector * (1.0 + scale_vector) + shift_vector).astype(jnp.bfloat16)


def fold_block(running, queries, keys_in, values_in, key_flags, bias_table, score_scale):
    run_max, run_total, summed = running
    scores = (
        jnp.einsum("qhmd,khmd->hmqk", queries, keys_in, preferred_element_type=jnp.float32)
        * score_scale
    )
    if key_flags is not None:
        scores = scores + bias_table[:, :, None, None] * key_flags
    new_max = jnp.maximum(run_max, jnp.max(scores, axis=-1))
    shrink = jnp.exp(run_max - new_max)
    weights = jnp.exp(scores - new_max[..., None])
    run_total = run_total * shrink + jnp.sum(weights, axis=-1)
    summed = summed * shrink[..., None] + jnp.einsum(
        "hmqk,khe->hmqe",
        weights.astype(jnp.bfloat16),
        values_in,
        preferred_element_type=jnp.float32,
    )
    return (new_max, run_total, summed)


def fold_keys(running, queries, keys_in, values_in, key_flags, bias_table, score_scale):
    full_blocks = keys_in.shape[0] // KEY_BLOCK
    if full_blocks > 1:
        edge = full_blocks * KEY_BLOCK
        stacked = (
            keys_in.reshape((full_blocks, KEY_BLOCK) + keys_in.shape[1:]),
            values_in.reshape((full_blocks, KEY_BLOCK) + values_in.shape[1:]),
        )

        def fold_step(current, block_data):
            flag_part = None
            return (
                fold_block(
                    current,
                    queries,
                    block_data[0],
                    block_data[1],
                    flag_part,
                    bias_table,
                    score_scale,
                ),
                None,
            )

        running, ignored = lax.scan(fold_step, running, stacked)
        keys_in = keys_in[edge:]
        values_in = values_in[edge:]
        key_flags = None
    if keys_in.shape[0] > 0:
        running = fold_block(
            running, queries, keys_in, values_in, key_flags, bias_table, score_scale
        )
    return running


def body(
    latent,
    condition,
    context,
    context_vector,
    modulator,
    norm_gain,
    query_weight,
    key_weight,
    value_weight,
    head_gain,
    lambdas,
    context_bias,
    out_weight,
):
    model_width = latent.shape[2]
    local_heads = lambdas.shape[0]
    query_width = query_weight.shape[1]
    head_size = query_width // (2 * local_heads)
    value_size = value_weight.shape[1] // local_heads
    score_scale = head_size ** (-0.5)
    activated = jax.nn.silu(
        jnp.concatenate([condition, context_vector[None, :]], axis=0).astype(jnp.float32)
    )
    partial_terms = jnp.dot(
        activated.astype(jnp.bfloat16), modulator, preferred_element_type=jnp.float32
    )
    modulations = by_axis(partial_terms, SP_TP)
    hidden = modulate(
        latent[0],
        norm_gain,
        modulations[0, :model_width],
        modulations[0, model_width : 2 * model_width],
    )
    ctx_hidden = modulate(
        context[0],
        norm_gain,
        modulations[1, :model_width],
        modulations[1, model_width : 2 * model_width],
    )
    gate_vector = modulations[0, 2 * model_width :]
    incoming = gather_directly(hidden, "tp", 0)
    projected = jnp.concatenate(
        [
            jnp.dot(incoming, query_weight, preferred_element_type=jnp.float32),
            jnp.dot(incoming, key_weight, preferred_element_type=jnp.float32),
            jnp.dot(incoming, value_weight, preferred_element_type=jnp.float32),
        ],
        axis=1,
    ).astype(jnp.bfloat16)
    query_rows = projected.shape[0]
    queries = projected[:, :query_width].reshape(query_rows, local_heads, 2, head_size)
    own_keys = projected[:, query_width : 2 * query_width]
    own_values = projected[:, 2 * query_width :]
    ctx_keys = jnp.dot(ctx_hidden, key_weight, preferred_element_type=jnp.float32).astype(
        jnp.bfloat16
    )
    ctx_values = jnp.dot(ctx_hidden, value_weight, preferred_element_type=jnp.float32).astype(
        jnp.bfloat16
    )
    ctx_keys, ctx_values = sent_together((ctx_keys, ctx_values), SP, 0, 1)
    start_carry = (
        jnp.full((local_heads, 2, query_rows), LOW_START, jnp.float32),
        jnp.zeros((local_heads, 2, query_rows), jnp.float32),
        jnp.zeros((local_heads, 2, query_rows, value_size), jnp.float32),
    )
    pieces = (own_keys, own_values)
    initial = fold_keys(
        start_carry,
        queries,
        ctx_keys.reshape(-1, local_heads, 2, head_size),
        ctx_values.reshape(-1, local_heads, value_size),
        jnp.ones((ctx_keys.shape[0],), jnp.float32),
        context_bias,
        score_scale,
    )
    incoming = sent_together((pieces[0], pieces[1]), SP, 0, 1)
    run_max, run_total, summed = fold_keys(
        initial,
        queries,
        incoming[0].reshape(-1, local_heads, 2, head_size),
        incoming[1].reshape(-1, local_heads, value_size),
        None,
        context_bias,
        score_scale,
    )
    mixed = (
        summed[:, 0] / run_total[:, 0, :, None]
        - lambdas[:, None, None] * summed[:, 1] / run_total[:, 1, :, None]
    )
    normed = (
        mixed
        * lax.rsqrt(jnp.mean(mixed * mixed, axis=-1, keepdims=True) + EPSILON)
        * head_gain
        * OUT_SCALE
    )
    attended = (
        jnp.transpose(normed, (1, 0, 2))
        .reshape(query_rows, local_heads * value_size)
        .astype(jnp.bfloat16)
    )
    branch = summed_on_arrival(
        jnp.dot(attended, out_weight, preferred_element_type=jnp.float32).astype(jnp.bfloat16),
        "tp",
        0,
    )
    result = (latent[0].astype(jnp.float32) + gate_vector * branch).astype(jnp.bfloat16)
    return result[None]


def solution(mesh):
    torus = Mesh(
        mesh.devices.reshape(8, 8, mesh.shape["tp"], mesh.shape["dp"]), ("sp_0", "sp_1", "tp", "dp")
    )
    return jax.shard_map(
        body,
        mesh=torus,
        in_specs=(
            P("dp", SP_TP, None),
            P("dp", SP_TP),
            P("dp", SP, None),
            P(SP_TP),
            P(SP_TP, None),
            P(),
            P(None, "tp"),
            P(None, "tp"),
            P(None, "tp"),
            P(),
            P("tp"),
            P("tp", None),
            P("tp", None),
        ),
        out_specs=P("dp", SP_TP, None),
        check_vma=False,
    )
```

profile of v0, /device:TPU:8, one launch (start us, length us, event | category | flops | bytes accessed | tf_op | source)
XLA Modules:
  0.0 289.6 jit_solution(1332967432429290090)
XLA Ops:
  7.8 36.4 %psum.21 = f32[2,6144]{1,0:T(2,128)S(1)} all-reduce(f32[2,6144]{1,0:T(2,128)S(1)} %fusion.60), channel_id=1, replica_groups=mesh['sp_0'=8,'sp_1'=8,'tp'=4,'dp'=2] {'sp_0'}, use_global_device_ids=true, to_apply=%region_0.1 | all-reduce | flops 12288 | bytes 98304 | tf_op jit(solution)/shard_map/psum | solution.py:19
  44.2 28.8 %psum.22 = f32[2,6144]{1,0:T(2,128)S(1)} all-reduce(f32[2,6144]{1,0:T(2,128)S(1)} %psum.21), channel_id=1, replica_groups=mesh['sp_0'=8,'sp_1'=8,'tp'=4,'dp'=2] {'sp_1'}, use_global_device_ids=true, to_apply=%region_1.2 | all-reduce | flops 12288 | bytes 98304 | tf_op jit(solution)/shard_map/psum | solution.py:19
  72.9 17.9 %psum.23 = f32[2,6144]{1,0:T(2,128)S(1)} all-reduce(f32[2,6144]{1,0:T(2,128)S(1)} %psum.22), channel_id=1, replica_groups=mesh['sp_0'=8,'sp_1'=8,'tp'=4,'dp'=2] {'tp'}, use_global_device_ids=true, to_apply=%region_2.3 | all-reduce | flops 12288 | bytes 98304 | tf_op jit(solution)/shard_map/psum | solution.py:19
  93.3 13.5 %all_to_all.10 = bf16[4,64,2048]{2,1,0:T(8,128)(2,1)S(1)} all-to-all(bf16[4,64,2048]{2,1,0:T(8,128)(2,1)S(1)} %broadcast_in_dim.13), channel_id=1, replica_groups=mesh['sp_0'=8,'sp_1'=8,'tp'=4,'dp'=2] {'tp'}, dimensions={0} | all-to-all | bytes 2097152 | tf_op jit(solution)/shard_map/all_to_all | solution.py:31
  109.1 49.1 %all_gather.6 = bf16[512,256]{1,0:T(8,128)(2,1)S(1)} all-gather(bf16[8,256]{1,0:T(8,128)(2,1)S(1)} %pad_maximum_fusion.1), channel_id=1, replica_groups=mesh['sp_0'=8,'sp_1'=8,'tp'=4,'dp'=2] {'sp_0','sp_1'}, dimensions={0}, use_global_device_ids=true | all-gather | bytes 266240 | tf_op jit(solution)/shard_map/all_gather | solution.py:44
  160.7 50.3 %all-gather.2.cloned.1.call-done = bf16[16384,256]{0,1:T(8,128)(2,1)} async-done(((bf16[256,256]{0,1:T(8,128)(2,1)}), bf16[16384,256]{0,1:T(8,128)(2,1)}) %all-gather.2.cloned.1.call-update) | async-done | bytes 8388624 | tf_op jit(solution)/shard_map/all_gather | solution.py:44
  211.0 5.0 %fusion.72 = (bf16[16384,128]{0,1:T(8,128)(2,1)}, bf16[16384,128]{0,1:T(8,128)(2,1)S(1)}) fusion(bf16[16384,256]{0,1:T(8,128)(2,1)} %all-gather.2.cloned.1.call-done), kind=kLoop, calls=%fused_computation.100 | loop fusion | bytes 16777216 | tf_op jit(solution)/shard_map/split | solution.py:44
  216.0 3.2 %copy.24 = bf16[16,8,8,2048]{3,2,1,0:T(8,128)(2,1)S(1)} copy(bf16[16,8,8,2048]{3,1,2,0:T(8,128)(2,1)S(1)} %bitcast.170) | data formatting | bytes 8388608
  219.2 4.2 %copy.20 = bf16[8,2048,1,2,64]{1,4,3,2,0:T(8,128)(2,1)} copy(bf16[8,2048,1,2,64]{1,0,4,3,2:T(8,128)(2,1)S(1)} %bitcast.166) | data formatting | bytes 8388608 | tf_op jit(solution)/shard_map/while | solution.py:110
  223.4 6.4 %copy.23 = bf16[16384,128]{1,0:T(8,128)(2,1)} copy(bf16[16384,128]{0,1:T(8,128)(2,1)} %get-tuple-element.77) | data formatting | bytes 8388608 | tf_op jit(solution)/shard_map/while | solution.py:110
  229.8 36.3 %while.14 = (s32[]{:T(128)}, f32[1,2,256]{2,1,0:T(2,128)S(1)}, f32[1,2,256]{2,1,0:T(2,128)S(1)}, f32[1,2,256,128]{3,2,1,0:T(8,128)S(1)}, bf16[8,2048,1,2,64]{1,4...) while((s32[]{:T(128)}, f32[1,2,256]{2,1,0:T(2,128)S(1)}, ...), condition=%wide.region_10.11_spmd, body=%wide.region_7.10_spmd.sunk | while | flops 411174400 | bytes 14255189 | solution.py:110
  231.6 2.0 fusion.97
  236.2 2.0 fusion.97
  240.7 2.0 fusion.97
  243.4 1.8 bitcast_reduce_fusion.2
  245.2 2.0 fusion.97
  247.9 1.8 bitcast_reduce_fusion.2
  249.8 2.0 fusion.97
  254.3 2.0 fusion.97
  257.0 1.8 bitcast_reduce_fusion.2
  258.9 2.0 fusion.97
  261.6 1.8 bitcast_reduce_fusion.2
  263.4 2.0 fusion.97
  266.9 14.9 %all_to_all.11 = bf16[4,64,2048]{2,1,0:T(8,128)(2,1)S(1)} all-to-all(bf16[4,64,2048]{2,1,0:T(8,128)(2,1)S(1)} %bitcast.172), channel_id=1, replica_groups=mesh['sp_0'=8,'sp_1'=8,'tp'=4,'dp'=2] {'tp'}, dimensions={0} | all-to-all | bytes 2097152 | tf_op jit(solution)/shard_map/all_to_all | solution.py:55
  (84 shorter events, 22.4 us)
Async XLA Ops:
  6.5 259.8 %copy-start = (bf16[128,2048]{1,0:T(8,128)(2,1)S(1)}, bf16[128,2048]{1,0:T(8,128)(2,1)}, u32[]{:S(2)}) copy-start(bf16[128,2048]{1,0:T(8,128)(2,1)} %param.27) | copy-start | bytes 1572868
  6.5 100.3 %copy-start.2 = (bf16[2048,128]{1,0:T(8,128)(2,1)S(1)}, bf16[2048,128]{1,0:T(8,128)(2,1)}, u32[]{:S(2)}) copy-start(bf16[2048,128]{1,0:T(8,128)(2,1)} %param.23) | copy-start | bytes 1572868
  6.5 100.8 %copy-start.3 = (bf16[2048,128]{1,0:T(8,128)(2,1)S(1)}, bf16[2048,128]{1,0:T(8,128)(2,1)}, u32[]{:S(2)}) copy-start(bf16[2048,128]{1,0:T(8,128)(2,1)} %param.22) | copy-start | bytes 1572868
  6.5 204.4 %all-gather.2.cloned.1.call-start = ((), (), s32[]{:S(2)}) async-start(), calls=%async_computation.2 | async-start | bytes 8519680 | tf_op jit(solution)/shard_map/all_gather | solution.py:44
  6.5 102.0 %copy-start.5 = (bf16[1,8,2048]{2,1,0:T(8,128)(2,1)S(1)}, bf16[1,8,2048]{2,1,0:T(8,128)(2,1)}, u32[]{:S(2)}) copy-start(bf16[1,8,2048]{2,1,0:T(8,128)(2,1)} %param.17) | copy-start | bytes 98308
  7.8 100.9 %copy-start.6 = (f32[2048]{0:T(1024)S(1)}, f32[2048]{0:T(1024)}, u32[]{:S(2)}) copy-start(f32[2048]{0:T(1024)} %param.20) | copy-start | bytes 24580
  93.3 65.7 %copy-start.4 = (bf16[2048,128]{1,0:T(8,128)(2,1)S(1)}, bf16[2048,128]{1,0:T(8,128)(2,1)}, u32[]{:S(2)}) copy-start(bf16[2048,128]{1,0:T(8,128)(2,1)} %param.21) | copy-start | bytes 1572868
  93.3 66.2 %copy-start.7 = (f32[1,2]{1,0:T(1,128)S(1)}, f32[1,2]{1,0:T(1,128)}, u32[]{:S(2)}) copy-start(f32[1,2]{1,0:T(1,128)} %param.26) | copy-start | bytes 28
  229.8 36.6 %copy-start.8 = (f32[128]{0:T(128)S(1)}, f32[128]{0:T(128)}, u32[]{:S(2)}) copy-start(f32[128]{0:T(128)} %param.24) | copy-start | bytes 1540
  266.1 15.9 %copy-start.1 = (bf16[1,64,2048]{2,1,0:T(8,128)(2,1)S(1)}, bf16[1,64,2048]{2,1,0:T(8,128)(2,1)}, u32[]{:S(2)}) copy-start(bf16[1,64,2048]{2,1,0:T(8,128)(2,1)} %param.15) | copy-start | bytes 786436
Sparse Core Ops, SparseCore 0:
  108.6 102.3 all-gather.1
where the time goes:
time: 291 us; the launch traced here: 290 us
  blocking collectives  161 us (55%)
  waiting for transfers between devices  50.3 us (17%)
  matrix products  34.6 us (12%)
  local copies, waits for them, and re-layouts  19.1 us (7%)
  between operations  14.3 us (5%)
  other arithmetic  10.4 us (4%)
    psum x3, blocking collectives, by_axis(): shard = lax.psum(shard, axis)  83.1 us
    all_gather x1, waiting for transfers between devices, sent_together(): lax.all_gather(both, axis, axis=dim, tiled=True)  50.3 us
    all_gather x1, blocking collectives, sent_together(): lax.all_gather(both, axis, axis=dim, tiled=True)  49.1 us
    dot_general x9, matrix products, fold_block(): jnp.einsum('hmqk,khe->hmqe', weights.astype(jnp.bfloat16), values_in, pre...  16 us
    dot_general x9, matrix products, fold_block(): jnp.einsum('qhmd,khmd->hmqk', queries, keys_in, preferred_element_type=jn...  14.9 us
    all_to_all x1, blocking collectives, summed_on_arrival(): lax.all_to_all(blocks, axis, split_axis=0, concat_axis=0, tiled=True)  14.9 us
    all_to_all x1, blocking collectives, sent_to_all(): return lax.all_to_all(copies, axis, split_axis=0, concat_axis=0, tiled=True)  13.5 us
    while x2, local copies, waits for them, and re-layouts, fold_keys(): running, ignored = lax.scan(fold_step, running, stacked)  10.6 us
  transfers between devices with their start and end apart: 1, of which 1 were waited for; matrix products, arithmetic and copies ran while one was open for 1% of the time, Pallas kernels for 0%

commit v1 on v0

v1 whole, which is shorter than its diff:
```python
import jax
import jax.numpy as jnp
from jax import lax
from jax.experimental import pallas as pl
from jax.experimental.pallas import tpu as pltpu
from jax.sharding import Mesh
from jax.sharding import PartitionSpec as P

SP_TP = ("sp_0", "sp_1", "tp")
SP = ("sp_0", "sp_1")
AXES = ("sp_1", "sp_0")

EPSILON = 1e-06
OUT_SCALE = 0.8
LOG2E = 1.4426950408889634

D = 2048
HEAD = 64
VAL = 128
ROWS = 64
NX = 4
NR = 8
BLOCK = ROWS * NX
CTX = 8
TALL = BLOCK + 2 * CTX
CHUNK = 3 * D // NX
MESH_ID = pl.DeviceIdType.MESH
NT = (((1,), (1,)), ((), ()))
F32 = jnp.float32
BF16 = jnp.bfloat16


def dot(a, b):
    return jnp.dot(a, b, preferred_element_type=F32)


def slot_left(d):
    return 8 - 2 * d


def slot_right(d):
    return 7 - 2 * d


def kernel(
    latent,
    condition,
    context,
    context_vector,
    modulator,
    norm_gain,
    query_weight,
    key_weight,
    value_weight,
    head_gain,
    lambdas,
    context_bias,
    out_weight,
    out,
    mod_v,
    part,
    xrs,
    ysum,
    zsum,
    xag,
    lat,
    ctx_v,
    gain_v,
    hgain_v,
    w_v,
    ow,
    normed_v,
    hidden_v,
    gx,
    gv,
    kctx,
    vctx,
    s_v,
    so,
    sl,
    ro,
    rl,
    att,
    attr,
    res,
    local_sem,
    mod_send,
    mod_recv,
    lat_send,
    lat_recv,
    ow_send,
    ow_recv,
    ring_send,
    ring_recv,
    o_send,
    o_recv,
    l_send,
    l_recv,
    a_send,
    a_recv,
):
    z = lax.axis_index("sp_0")
    y = lax.axis_index("sp_1")
    x = lax.axis_index("tp")
    place = (y, z)

    def remote(src, dst, send, recv, axis, target):
        return pltpu.make_async_remote_copy(
            src_ref=src,
            dst_ref=dst,
            send_sem=send,
            recv_sem=recv,
            device_id={axis: target},
            device_id_type=MESH_ID,
        )

    barrier = pltpu.get_barrier_semaphore()
    for d in range(1, NX):
        pl.semaphore_signal(
            barrier, inc=1, device_id={"tp": lax.rem(x + d, NX)}, device_id_type=MESH_ID
        )
    for axis, here in zip(AXES, place):
        for d in range(1, NR):
            pl.semaphore_signal(
                barrier, inc=1, device_id={axis: lax.rem(here + d, NR)}, device_id_type=MESH_ID
            )

    loads = {
        "mod": pltpu.make_async_copy(modulator, mod_v, local_sem.at[0]),
        "lat": pltpu.make_async_copy(latent.at[0], lat.at[x], local_sem.at[1]),
        "ctx": pltpu.make_async_copy(context.at[0], ctx_v, local_sem.at[2]),
        "gain": pltpu.make_async_copy(norm_gain, gain_v, local_sem.at[3]),
        "hgain": pltpu.make_async_copy(head_gain, hgain_v, local_sem.at[4]),
        "q": pltpu.make_async_copy(query_weight, w_v.at[:, pl.ds(0, VAL)], local_sem.at[5]),
        "k": pltpu.make_async_copy(key_weight, w_v.at[:, pl.ds(VAL, VAL)], local_sem.at[6]),
        "v": pltpu.make_async_copy(value_weight, w_v.at[:, pl.ds(2 * VAL, VAL)], local_sem.at[7]),
        "ow": pltpu.make_async_copy(out_weight, ow.at[x], local_sem.at[8]),
    }
    for name in loads:
        loads[name].start()

    loads["mod"].wait()
    vectors = jnp.concatenate(
        [condition[...].astype(F32), context_vector[...].astype(F32)], axis=0
    )
    activated = (vectors / (1.0 + jnp.exp(-vectors))).astype(BF16).astype(F32)
    for c in range(NX):
        terms = dot(activated, mod_v[:, c * CHUNK : (c + 1) * CHUNK].astype(F32))
        part[c] = terms
    xrs[x] = part[x]
    loads["lat"].wait()

    pl.semaphore_wait(barrier, NX - 1 + 2 * (NR - 1))

    first = []
    for d in range(1, NX):
        to = lax.rem(x + d, NX)
        first.append(remote(part.at[to], xrs.at[x], mod_send.at[d], mod_recv.at[d], "tp", to))
    for copy in first:
        copy.start()

    right, left = lax.rem(x + 1, NX), lax.rem(x + NX - 1, NX)
    far = lax.rem(x + 2, NX)
    half = ROWS // 2
    lat_right = remote(lat.at[x], lat.at[x], lat_send.at[0], lat_recv.at[0], "tp", right)
    lat_left = remote(lat.at[x], lat.at[x], lat_send.at[1], lat_recv.at[1], "tp", left)
    lat_right.start()
    lat_left.start()

    for copy in first:
        copy.wait()
    ysum[y] = xrs[0] + xrs[1] + xrs[2] + xrs[3]

    second = []
    for d in range(1, NR):
        to = lax.rem(y + d, NR)
        second.append(
            remote(ysum.at[y], ysum.at[y], mod_send.at[8 + d], mod_recv.at[8 + d], "sp_1", to)
        )
    for copy in second:
        copy.start()
    for copy in second:
        copy.wait()
    zsum[z] = jnp.sum(ysum[...], axis=0)
    third = []
    for d in range(1, NR):
        to = lax.rem(z + d, NR)
        third.append(
            remote(zsum.at[z], zsum.at[z], mod_send.at[16 + d], mod_recv.at[16 + d], "sp_0", to)
        )
    for copy in third:
        copy.start()

    lat_right.wait()
    relay_right = remote(
        lat.at[left, pl.ds(0, half)],
        lat.at[left, pl.ds(0, half)],
        lat_send.at[2],
        lat_recv.at[2],
        "tp",
        right,
    )
    relay_right.start()
    lat_left.wait()
    relay_left = remote(
        lat.at[right, pl.ds(half, half)],
        lat.at[right, pl.ds(half, half)],
        lat_send.at[3],
        lat_recv.at[3],
        "tp",
        left,
    )
    relay_left.start()

    def normalise(rows):
        as_float = rows.astype(F32)
        return as_float * lax.rsqrt(
            jnp.mean(as_float * as_float, axis=-1, keepdims=True) + EPSILON
        )

    def normalise_block(b):
        base = pl.multiple_of(b * ROWS, ROWS)
        normed_v[pl.ds(base, ROWS), :] = normalise(lat[b])

    normalise_block(x)
    normalise_block(left)
    normalise_block(right)
    loads["ctx"].wait()
    normed_v[pl.ds(BLOCK, CTX), :] = normalise(ctx_v[...])

    for copy in third:
        copy.wait()
    xag[x] = jnp.sum(zsum[...], axis=0)
    fourth = []
    for d in range(1, NX):
        to = lax.rem(x + d, NX)
        fourth.append(
            remote(xag.at[x], xag.at[x], mod_send.at[24 + d], mod_recv.at[24 + d], "tp", to)
        )
    for copy in fourth:
        copy.start()

    loads["ow"].wait()
    ow_right = remote(ow.at[x], ow.at[x], ow_send.at[0], ow_recv.at[0], "tp", right)
    ow_left = remote(ow.at[x], ow.at[x], ow_send.at[1], ow_recv.at[1], "tp", left)
    ow_right.start()
    ow_left.start()

    relay_right.wait()
    relay_left.wait()
    normalise_block(far)
    for name in ("gain", "q", "k", "v", "hgain"):
        loads[name].wait()
    for copy in fourth:
        copy.wait()

    def modulation(row, first_lane):
        pieces = []
        at = first_lane
        while at < first_lane + D:
            c = at // CHUNK
            stop = min(first_lane + D, (c + 1) * CHUNK)
            pieces.append(xag[c, row : row + 1, at - c * CHUNK : stop - c * CHUNK])
            at = stop
        return jnp.concatenate(pieces, axis=1)

    gain = gain_v[...]
    multiplier = gain * (1.0 + modulation(0, D))
    shift = modulation(0, 0)

    for b in range(NX):
        rows = slice(b * ROWS, (b + 1) * ROWS)
        hidden_v[rows, :] = (normed_v[rows, :] * multiplier + shift).astype(BF16)
    ctx_hidden = normed_v[BLOCK : BLOCK + CTX, :] * (
        gain * (1.0 + modulation(1, D))
    ) + modulation(1, 0)
    hidden_v[BLOCK:TALL, :] = jnp.concatenate(
        [ctx_hidden, jnp.zeros_like(ctx_hidden)], axis=0
    ).astype(BF16)

    projected = dot(hidden_v[...], w_v[...])
    q = projected[:BLOCK, :VAL] * (HEAD ** (-0.5) * LOG2E)
    k = projected[:BLOCK, VAL : 2 * VAL]
    v = projected[:BLOCK, 2 * VAL :]
    low = lax.broadcasted_iota(jnp.int32, (BLOCK, VAL), 1) < HEAD
    own = NR - 1
    tail = jnp.concatenate(
        [projected[BLOCK : BLOCK + CTX, VAL : 2 * VAL], projected[BLOCK : BLOCK + CTX, 2 * VAL :]],
        axis=0,
    )
    gx[0, own] = jnp.concatenate([jnp.where(low, k, q), tail], axis=0).astype(BF16)
    gx[1, own] = jnp.concatenate([jnp.where(low, q, k), tail], axis=0).astype(BF16)
    transposed = jnp.transpose(v).astype(BF16)
    gv[0, own] = transposed
    gv[1, own] = transposed

    def ring_copies(a, step):
        axis, here = AXES[a], place[a]
        to_right, to_left = lax.rem(here + 1, NR), lax.rem(here + NR - 1, NR)
        from_left = own if step == 0 else slot_left(step)
        from_right = own if step == 0 else slot_right(step)
        last = step == NR // 2 - 1
        copies = []
        for part_index, buffer in ((0, gx), (1, gv)):
            if not (last and part_index == 1):
                at = ((a * 2) * 4 + step) * 2 + part_index
                copies.append(
                    remote(
                        buffer.at[a, from_left],
                        buffer.at[a, slot_left(step + 1)],
                        ring_send.at[at],
                        ring_recv.at[at],
                        axis,
                        to_right,
                    )
                )
            if not (last and part_index == 0):
                at = ((a * 2 + 1) * 4 + step) * 2 + part_index
                copies.append(
                    remote(
                        buffer.at[a, from_right],
                        buffer.at[a, slot_left(NR // 2) if last else slot_right(step + 1)],
                        ring_send.at[at],
                        ring_recv.at[at],
                        axis,
                        to_left,
                    )
                )
        return copies

    rings = [[ring_copies(a, step) for step in range(4)] for a in range(2)]
    for a in range(2):
        for copy in rings[a][0]:
            copy.start()
    for step in range(1, 4):
        for index in range(4):
            for a in range(2):
                rings[a][step - 1][index].wait_recv()
                if step < 3:
                    rings[a][step][index].start()
                elif index == 0:
                    rings[a][3][0].start()
                elif index == 3:
                    rings[a][3][1].start()
    for a in range(2):
        for copy in rings[a][3]:
            copy.wait_recv()

    ow_right.wait()
    ow_left.wait()
    ow_half = VAL // 2
    ow_relay_right = remote(
        ow.at[left, pl.ds(0, ow_half)],
        ow.at[left, pl.ds(0, ow_half)],
        ow_send.at[2],
        ow_recv.at[2],
        "tp",
        right,
    )
    ow_relay_left = remote(
        ow.at[right, pl.ds(ow_half, ow_half)],
        ow.at[right, pl.ds(ow_half, ow_half)],
        ow_send.at[3],
        ow_recv.at[3],
        "tp",
        left,
    )
    ow_relay_right.start()
    ow_relay_left.start()

    for a in range(2):
        tails = [gx[a, j, BLOCK:TALL, :].astype(F32) for j in range(NR)]
        kctx[a] = jnp.concatenate([t[:CTX] for t in tails], axis=0).astype(BF16)
        rows = jnp.concatenate(
            [t[CTX:] for t in tails] + [jnp.zeros((VAL - NR * CTX, VAL), F32)], axis=0
        )
        vctx[a] = jnp.transpose(rows)[:, : NR * CTX].astype(BF16)

    lane = lax.broadcasted_iota(jnp.int32, (1, VAL), 1)
    is_low = jnp.where(lane < HEAD, 1.0, 0.0)
    masks = (is_low.astype(BF16), (1.0 - is_low).astype(BF16))

    def first_pass(a, t):
        masked = gx[1 - a, t, 0:BLOCK, :] * masks[a]
        top = None
        for j in range(NR):
            scores = lax.dot_general(
                gx[a, j, 0:BLOCK, :], masked, NT, preferred_element_type=F32
            )
            s_v[a, j * BLOCK : (j + 1) * BLOCK, :] = scores
            block_top = jnp.max(scores.reshape(BLOCK // 8, 8, BLOCK), axis=0)
            top = block_top if top is None else jnp.maximum(top, block_top)
            yield None
        ctx_scores = (
            lax.dot_general(kctx[a], masked, NT, preferred_element_type=F32)
            + context_bias[0, a] * LOG2E
        )
        top = jnp.maximum(top, jnp.max(ctx_scores.reshape(NR * CTX // 8, 8, BLOCK), axis=0))
        top = jnp.broadcast_to(jnp.max(top, axis=0, keepdims=True), (8, BLOCK))
        yield (top, ctx_scores)

    def second_pass(a, t, top, ctx_scores):
        weights = jnp.exp2(ctx_scores.reshape(NR * CTX // 8, 8, BLOCK) - top[None])
        total = jnp.sum(weights, axis=0)
        acc = dot(vctx[a], weights.reshape(NR * CTX, BLOCK).astype(BF16))
        for j in range(NR):
            scores = s_v[a, j * BLOCK : (j + 1) * BLOCK, :]
            weights = jnp.exp2(scores.reshape(BLOCK // 8, 8, BLOCK) - top[None])
            total = total + jnp.sum(weights, axis=0)
            acc = acc + dot(gv[a, j], weights.reshape(BLOCK, BLOCK).astype(BF16))
            yield None
        total = jnp.sum(total, axis=0, keepdims=True)
        so[a, t] = (acc * (1.0 / total)).astype(BF16)
        sl[a, t] = top[0:1] + jnp.log2(total)
        yield None

    def o_copies(a, t):
        axis, here = AXES[1 - a], place[1 - a]
        away = (NR // 2 - lax.div(t + 1, 2)) * (1 - 2 * lax.rem(t + 1, 2))
        to = lax.rem(here + away + NR, NR)
        return (
            remote(so.at[a, t], ro.at[a, t], o_send.at[a, t], o_recv.at[a, t], axis, to),
            remote(sl.at[a, t], rl.at[a, t], l_send.at[a, t], l_recv.at[a, t], axis, to),
        )

    def run(generators):
        last = [None] * len(generators)
        alive = list(range(len(generators)))
        while alive:
            for g in list(alive):
                try:
                    value = next(generators[g])
                    if value is not None:
                        last[g] = value
                except StopIteration:
                    alive.remove(g)
        return last

    def attend(t, carry):
        (found0,) = run([first_pass(0, t)])
        _, found1 = run([second_pass(0, t, *found0), first_pass(1, t)])
        run([second_pass(1, t, *found1)])

        @pl.when(t < own)
        def _():
            for a in range(2):
                for copy in o_copies(a, t):
                    copy.start()

        return carry

    lax.fori_loop(0, NR, attend, 0)

    for a in range(2):
        for step in range(4):
            for copy in rings[a][step]:
                copy.wait_send()

    outs = []
    for a in range(2):
        for t in range(own):
            for copy in o_copies(a, t):
                copy.wait()
        logs = [rl[a, t] for t in range(own)] + [sl[a, own]]
        top = logs[0]
        for value in logs[1:]:
            top = jnp.maximum(top, value)
        total = None
        merged = None
        for t in range(NR):
            weight = jnp.exp2(logs[t] - top)
            block = so[a, own] if t == own else ro[a, t]
            term = block.astype(F32) * weight
            total = weight if total is None else total + weight
            merged = term if merged is None else merged + term
        outs.append(merged * (1.0 / total))
    mixed = outs[0] - lambdas[0] * outs[1]
    mixed = mixed * lax.rsqrt(jnp.mean(mixed * mixed, axis=0, keepdims=True) + EPSILON)
    attended = (jnp.transpose(mixed) * (hgain_v[...] * OUT_SCALE)).astype(BF16)
    for b in range(NX):
        att[b] = attended[b * ROWS : (b + 1) * ROWS]
    attr[x] = att[x]
    fifth = []
    for d in range(1, NX):
        to = lax.rem(x + d, NX)
        fifth.append(remote(att.at[to], attr.at[x], a_send.at[d], a_recv.at[d], "tp", to))
    for copy in fifth:
        copy.start()
    ow_relay_right.wait()
    ow_relay_left.wait()
    for copy in fifth:
        copy.wait()

    joined = jnp.concatenate([attr[b] for b in range(NX)], axis=1)
    gate = modulation(0, 2 * D)
    width = 512
    for c in range(D // width):
        lanes = slice(c * width, (c + 1) * width)
        weights = jnp.concatenate([ow[b, :, lanes] for b in range(NX)], axis=0)
        branch = dot(joined, weights)
        res[:, lanes] = (lat[x, :, lanes].astype(F32) + gate[:, lanes] * branch).astype(BF16)
    done = pltpu.make_async_copy(res, out.at[0], local_sem.at[9])
    done.start()
    done.wait()


def body(
    latent,
    condition,
    context,
    context_vector,
    modulator,
    norm_gain,
    query_weight,
    key_weight,
    value_weight,
    head_gain,
    lambdas,
    context_bias,
    out_weight,
):
    anywhere = pl.BlockSpec(memory_space=pl.ANY)
    vmem = pl.BlockSpec(memory_space=pltpu.VMEM)
    smem = pl.BlockSpec(memory_space=pltpu.SMEM)
    dma = pltpu.SemaphoreType.DMA
    return pl.pallas_call(
        kernel,
        out_shape=jax.ShapeDtypeStruct(latent.shape, latent.dtype),
        in_specs=[
            anywhere,
            vmem,
            anywhere,
            vmem,
            anywhere,
            anywhere,
            anywhere,
            anywhere,
            anywhere,
            anywhere,
            smem,
            smem,
            anywhere,
        ],
        out_specs=anywhere,
        scratch_shapes=[
            pltpu.VMEM((8, 3 * D), BF16),
            pltpu.VMEM((NX, 2, CHUNK), F32),
            pltpu.VMEM((NX, 2, CHUNK), F32),
            pltpu.VMEM((NR, 2, CHUNK), F32),
            pltpu.VMEM((NR, 2, CHUNK), F32),
            pltpu.VMEM((NX, 2, CHUNK), F32),
            pltpu.VMEM((NX, ROWS, D), BF16),
            pltpu.VMEM((CTX, D), BF16),
            pltpu.VMEM((1, D), F32),
            pltpu.VMEM((1, VAL), F32),
            pltpu.VMEM((D, 3 * VAL), BF16),
            pltpu.VMEM((NX, VAL, D), BF16),
            pltpu.VMEM((TALL, D), F32),
            pltpu.VMEM((TALL, D), BF16),
            pltpu.VMEM((2, NR, TALL, VAL), BF16),
            pltpu.VMEM((2, NR, VAL, BLOCK), BF16),
            pltpu.VMEM((2, NR * CTX, VAL), BF16),
            pltpu.VMEM((2, VAL, NR * CTX), BF16),
            pltpu.VMEM((2, NR * BLOCK, BLOCK), F32),
            pltpu.VMEM((2, NR, VAL, BLOCK), BF16),
            pltpu.VMEM((2, NR, 1, BLOCK), F32),
            pltpu.VMEM((2, NR, VAL, BLOCK), BF16),
            pltpu.VMEM((2, NR, 1, BLOCK), F32),
            pltpu.VMEM((NX, ROWS, VAL), BF16),
            pltpu.VMEM((NX, ROWS, VAL), BF16),
            pltpu.VMEM((ROWS, D), BF16),
            dma((10,)),
            dma((32,)),
            dma((32,)),
            dma((4,)),
            dma((4,)),
            dma((4,)),
            dma((4,)),
            dma((32,)),
            dma((32,)),
            dma((2, NR)),
            dma((2, NR)),
            dma((2, NR)),
            dma((2, NR)),
            dma((4,)),
            dma((4,)),
        ],
        compiler_params=pltpu.CompilerParams(
            collective_id=0, has_side_effects=True, vmem_limit_bytes=60 * 1024 * 1024
        ),
    )(
        latent,
        condition,
        context,
        context_vector.reshape(1, -1),
        modulator,
        norm_gain.reshape(1, -1),
        query_weight,
        key_weight,
        value_weight,
        head_gain.reshape(1, -1),
        lambdas,
        context_bias,
        out_weight,
    )


def solution(mesh):
    torus = Mesh(
        mesh.devices.reshape(8, 8, mesh.shape["tp"], mesh.shape["dp"]), ("sp_0", "sp_1", "tp", "dp")
    )
    return jax.shard_map(
        body,
        mesh=torus,
        in_specs=(
            P("dp", SP_TP, None),
            P("dp", SP_TP),
            P("dp", SP, None),
            P(SP_TP),
            P(SP_TP, None),
            P(),
            P(None, "tp"),
            P(None, "tp"),
            P(None, "tp"),
            P(),
            P("tp"),
            P("tp", None),
            P("tp", None),
        ),
        out_specs=P("dp", SP_TP, None),
        check_vma=False,
    )
```

time: 291 us -> 78.7 us (0.27)
  the two profiles are of different devices: /device:TPU:8 before, /device:TPU:88 now
where the time goes in v1:
time: 78.7 us; the launch traced here: 78.5 us
  Pallas kernels  76.2 us (97%)
  local copies, waits for them, and re-layouts  1.67 us (2%)
    pallas_call x1, Pallas kernels, body(): pl.pallas_call(kernel, out_shape=jax.ShapeDtypeStruct(latent.shape, laten...  76.2 us
    unnamed x1, local copies, waits for them, and re-layouts  1.67 us

profile of v1, /device:TPU:88, one launch (start us, length us, event | category | flops | bytes accessed | tf_op | source)
XLA Modules:
  0.0 78.5 jit_solution(11956674458727424482)
XLA Ops:
  0.7 76.2 %shard_map.127 = bf16[1,64,2048]{2,1,0:T(8,128)(2,1)} custom-call(bf16[1,64,2048]{2,1,0:T(8,128)(2,1)} %latent.1, bf16[1,8]{1,0:T(2,128)(2,1)} %condition.1, bf16[1,8,2048]{2,1,0:T(8,128)(2,1)} %context.1, bf16[1,8]{1,0:T(2,128)(2,1)} %bitcast.4, bf16[8,6144]{1,0:T(8,128)(2,1)} %modulator.1, f32[1,2048]{1,0:T(1,128)} %bitcast.3, ...), custom_call_target="tpu_custom_call" | custom-call | tf_op jit(solution)/shard_map/pallas_call | solution.py:526
  76.8 1.7 %copy.16 = bf16[1,64,2048]{2,1,0:T(8,128)(2,1)} copy(bf16[1,64,2048]{2,1,0:T(8,128)(2,1)} %shard_map.127) | data formatting | bytes 524288
